TPU v7x, 32 devices: a whole 2x2x4 slice. The times are simulated.
32 devices in a mesh: grp: 2 (over y), sp: 4 (over z), tp: 4 (over x, core).
Axes of the slice: x: 2, y: 2, z: 4, core: 2. Of those that a mesh axis runs over, the one named last changes fastest.
Arguments:
- stream: bfloat16 [3072, 4096], P(('grp', 'sp'), 'tp'), parts along dimension 0, may hold values from -6 to 6
- norm_gain: bfloat16 [2, 4096], replicated, may hold values from 0.099609375 to 1.8984375
- w_signal: bfloat16 [2, 4096, 1024], P(None, 'sp', 'tp'), may hold values from -0.09375 to 0.09375
- w_gate: bfloat16 [2, 4096, 1024], P(None, 'sp', 'tp'), may hold values from -0.09375 to 0.09375
- conv_taps: bfloat16 [2, 31, 1024], P(None, None, 'tp'), may hold values from -4 to 4
- conv_bias: bfloat16 [2, 1024], P(None, 'tp'), may hold values from -3 to 3
- ln_gain: bfloat16 [2, 1024], P(None, 'tp'), may hold values from 0.099609375 to 1.8984375
- ln_shift: bfloat16 [2, 1024], P(None, 'tp'), may hold values from -3 to 3
- w_out: bfloat16 [2, 1024, 4096], P(None, 'sp', 'tp'), may hold values from -0.375 to 0.375
Outputs:
- mixed_stream: bfloat16 [3072, 4096], P(('grp', 'sp'), 'tp'), parts along dimension 0
There are 2 independent parts, one for each index of `grp`. A program takes and returns all parts, laid end to end along the dimension named above; an argument that names none is the same for every part. Nothing has to cross between parts.
All inputs are finite; a program needn't handle non-finite values.
Results may differ from a plain program's by a relative error of at most 0.01.
Values may be sent and summed in bfloat16 or wider, within the bound.
A program may use at most 64 MiB of HBM per device.

v0:
```python
import jax
import jax.numpy as jnp
from jax import lax
from jax.sharding import PartitionSpec as P

C = 1024
EPS = 1e-05


def shifted(value, axis, steps):
    count = lax.axis_size(axis)
    initial, last = (max(0, -steps), min(count, count - steps))
    return lax.ppermute(value, axis, [(source, source + steps) for source in range(initial, last)])


def product(left, right):
    return jnp.dot(left, right, preferred_element_type=jnp.float32)


def shards(stream, norm_gain, w_signal, w_gate, conv_taps, conv_bias, ln_gain, ln_shift, w_out):
    fringe_rows = conv_taps.shape[1] - 1
    own_rows = stream.shape[0]
    layer_count = w_signal.shape[0]
    local_channels = w_signal.shape[2]
    whole_signal, whole_gate, whole_out = (
        lax.all_gather(w_signal, "sp", axis=1, tiled=True),
        lax.all_gather(w_gate, "sp", axis=1, tiled=True),
        lax.all_gather(w_out, "sp", axis=1, tiled=True),
    )
    current = stream
    for layer_index in range(layer_count):
        features = lax.all_gather(current, "tp", axis=1, tiled=True)
        widened = features.astype(jnp.float32)
        normed = (
            widened
            * lax.rsqrt(jnp.mean(widened * widened, axis=-1, keepdims=True) + EPS)
            * norm_gain[layer_index].astype(jnp.float32)
        ).astype(jnp.bfloat16)
        signal = product(normed, whole_signal[layer_index])
        gate_pre = product(normed, whole_gate[layer_index])
        blended = (signal * jax.nn.sigmoid(gate_pre)).astype(jnp.bfloat16)
        earlier = shifted(blended[own_rows - fringe_rows :], "sp", 1)
        padded = jnp.concatenate([earlier, blended], axis=0)
        length = padded.shape[0] - fringe_rows
        filtered = jnp.zeros((length, local_channels), jnp.float32) + conv_bias[layer_index].astype(
            jnp.float32
        )
        tap_rows = conv_taps[layer_index].astype(jnp.float32)
        for tap_index in range(fringe_rows + 1):
            filtered = filtered + tap_rows[tap_index] * padded[
                tap_index : tap_index + length
            ].astype(jnp.float32)
        totals = lax.psum((jnp.sum(filtered, axis=-1), jnp.sum(filtered * filtered, axis=-1)), "tp")
        average = totals[0][:, None] / C
        spread = totals[1][:, None] / C - average * average
        scaled = (filtered - average) * lax.rsqrt(spread + EPS) * ln_gain[layer_index].astype(
            jnp.float32
        ) + ln_shift[layer_index].astype(jnp.float32)
        activated = jax.nn.silu(scaled).astype(jnp.bfloat16)
        channels = lax.all_gather(activated, "tp", axis=1, tiled=True)
        update = product(channels, whole_out[layer_index])
        current = (current.astype(jnp.float32) + update).astype(jnp.bfloat16)
    return current


def solution(mesh):
    return jax.shard_map(
        shards,
        mesh=mesh,
        in_specs=(
            P(("grp", "sp"), "tp"),
            P(),
            P(None, "sp", "tp"),
            P(None, "sp", "tp"),
            P(None, None, "tp"),
            P(None, "tp"),
            P(None, "tp"),
            P(None, "tp"),
            P(None, "sp", "tp"),
        ),
        out_specs=P(("grp", "sp"), "tp"),
        check_vma=False,
    )
```

profile of v0, /device:TPU:0, one launch (start us, length us, event | category | flops | bytes accessed | tf_op | source)
XLA Modules:
  0.0 354.0 jit_solution(9451302702197944775)
XLA Ops:
  6.5 0.7 all-gather.6.cloned.1.call-update
  7.3 0.7 all-gather.10.cloned.1.call-update
  8.1 0.7 all-gather.8.cloned.1.call-update
  8.8 0.5 all-gather.12.cloned.1.call-update
  9.4 0.8 slice_convert_fusion.6
  10.1 0.8 slice_convert_fusion.5
  10.9 0.9 slice_convert_fusion
  11.8 0.8 slice_convert_fusion.2
  12.6 27.5 %all-gather.6.cloned.1.call-done = bf16[384,4096]{1,0:T(8,128)(2,1)} async-done(((bf16[384,1024]{1,0:T(8,128)(2,1)}), bf16[384,4096]{1,0:T(8,128)(2,1)}) %all-gather.6.cloned.1.call-update) | async-done | bytes 3145744 | tf_op jit(solution)/shard_map/all_gather | solution.py:32
  40.2 2.6 fusion
  42.7 79.8 %all-gather.10.cloned.1.call-done = bf16[2,4096,256]{2,1,0:T(8,128)(2,1)} async-done(((bf16[2,1024,256]{2,1,0:T(8,128)(2,1)}), bf16[2,4096,256]{2,1,0:T(8,128)(2,1)}) %all-gather.10.cloned.1.call-update) | async-done | bytes 4194320 | tf_op jit(solution)/shard_map/all_gather | solution.py:27
  122.5 4.5 %fusion.21 = f32[384,256]{1,0:T(8,128)} fusion(bf16[2,4096,256]{2,1,0:T(8,128)(2,1)} %all-gather.10.cloned.1.call-done, bf16[384,4096]{1,0:T(8,128)(2,1)} %all-gather.6.cloned.1.call-done, f32[4096]{0:T(1024)S(1)} %bitcast.120, f32[384]{0:T(512)S(1)} %add_rsqrt_fusion.3), kind=kOutput, calls=%fused_computation.91 | convolution fusion | flops 811892736 | bytes 5654016 | tf_op jit(solution)/shard_map/dot_general | solution.py:17
  127.0 76.4 %all-gather.8.cloned.1.call-done = bf16[2,4096,256]{2,1,0:T(8,128)(2,1)} async-done(((bf16[2,1024,256]{2,1,0:T(8,128)(2,1)}), bf16[2,4096,256]{2,1,0:T(8,128)(2,1)}) %all-gather.8.cloned.1.call-update) | async-done | bytes 4194320 | tf_op jit(solution)/shard_map/all_gather | solution.py:26
  203.3 2.8 fusion.23
  206.1 1.3 collective-permute-start
  207.4 1.4 collective-permute-done
  208.8 1.9 fusion.87
  210.7 5.9 %all-reduce.1 = (f32[384]{0:T(512)S(1)}, f32[384]{0:T(512)S(1)}) all-reduce(f32[384]{0:T(512)S(1)} %get-tuple-element.8, f32[384]{0:T(512)S(1)} %get-tuple-element.7), channel_id=1, replica_groups=mesh['grp'=2,'sp'=4,'tp'=4] {'tp'}, use_global_device_ids=true, to_apply=%region_4.0 | all-reduce | flops 768 | bytes 6144 | tf_op jit(solution)/shard_map/psum | solution.py:53
  216.8 8.8 %all_gather.24 = bf16[384,1024]{1,0:T(8,128)(2,1)S(1)} all-gather(bf16[384,256]{1,0:T(8,128)(2,1)S(1)} %multiply_convert_fusion.1), channel_id=1, replica_groups=mesh['grp'=2,'sp'=4,'tp'=4] {'tp'}, dimensions={1}, use_global_device_ids=true | all-gather | bytes 983040 | tf_op jit(solution)/shard_map/all_gather | solution.py:60
  225.6 58.4 %all-gather.12.cloned.1.call-done = bf16[2,1024,1024]{2,1,0:T(8,128)(2,1)} async-done(((bf16[2,256,1024]{2,1,0:T(8,128)(2,1)}), bf16[2,1024,1024]{2,1,0:T(8,128)(2,1)}) %all-gather.12.cloned.1.call-update) | async-done | bytes 4194320 | tf_op jit(solution)/shard_map/all_gather | solution.py:28
  284.0 3.6 %add_convert_fusion.1 = bf16[384,1024]{1,0:T(8,128)(2,1)} fusion(bf16[384,1024]{1,0:T(8,128)(2,1)} %param.9, bf16[384,1024]{1,0:T(8,128)(2,1)S(1)} %all_gather.24, bf16[2,1024,1024]{2,1,0:T(8,128)(2,1)} %all-gather.12.cloned.1.call-done), kind=kOutput, calls=%fused_computation.81 | convolution fusion | flops 806486016 | bytes 4456448 | tf_op jit(solution)/shard_map/dot_general | solution.py:17
  287.7 27.1 %all-gather.14.cloned.1.call-done = bf16[384,4096]{1,0:T(8,128)(2,1)} async-done(((bf16[384,1024]{1,0:T(8,128)(2,1)}), bf16[384,4096]{1,0:T(8,128)(2,1)}) %all-gather.14.cloned.1.call-update) | async-done | bytes 3145744 | tf_op jit(solution)/shard_map/all_gather | solution.py:32
  314.8 2.6 fusion.3
  317.4 3.7 %fusion.19 = f32[384,256]{1,0:T(8,128)S(1)} fusion(bf16[2,4096,256]{2,1,0:T(8,128)(2,1)} %all-gather.10.cloned.1.call-done, bf16[384,4096]{1,0:T(8,128)(2,1)} %all-gather.14.cloned.1.call-done, f32[4096]{0:T(1024)S(1)} %bitcast.118, f32[384]{0:T(512)S(1)} %add_rsqrt_fusion.1), kind=kOutput, calls=%fused_computation.89 | convolution fusion | flops 811892736 | bytes 5654016 | tf_op jit(solution)/shard_map/dot_general | solution.py:17
  321.2 1.0 copy-done.4
  322.1 1.0 fusion.22
  323.2 3.4 collective-permute-start.1
  326.6 1.4 collective-permute-done.1
  328.0 1.9 fusion.86
  329.9 5.9 %all-reduce = (f32[384]{0:T(512)S(1)}, f32[384]{0:T(512)S(1)}) all-reduce(f32[384]{0:T(512)S(1)} %get-tuple-element.6, f32[384]{0:T(512)S(1)} %get-tuple-element.5), channel_id=1, replica_groups=mesh['grp'=2,'sp'=4,'tp'=4] {'tp'}, use_global_device_ids=true, to_apply=%region_9.10 | all-reduce | flops 768 | bytes 6144 | tf_op jit(solution)/shard_map/psum | solution.py:53
  336.1 7.9 %all_gather.27 = bf16[384,1024]{1,0:T(8,128)(2,1)S(1)} all-gather(bf16[384,256]{1,0:T(8,128)(2,1)S(1)} %multiply_convert_fusion), channel_id=1, replica_groups=mesh['grp'=2,'sp'=4,'tp'=4] {'tp'}, dimensions={1}, use_global_device_ids=true | all-gather | bytes 983040 | tf_op jit(solution)/shard_map/all_gather | solution.py:60
  344.1 3.5 add_convert_fusion
  (28 shorter events, 0.7 us)
Async XLA Ops:
  6.5 33.6 %all-gather.6.cloned.1.call-start = ((), (), s32[]{:S(2)}) async-start(), calls=%async_computation | async-start | bytes 3932160 | tf_op jit(solution)/shard_map/all_gather | solution.py:32
  7.3 115.2 %all-gather.10.cloned.1.call-start = ((), (), s32[]{:S(2)}) async-start(), calls=%async_computation.2 | async-start | bytes 5242880 | tf_op jit(solution)/shard_map/all_gather | solution.py:27
  8.0 195.3 %all-gather.8.cloned.1.call-start = ((), (), s32[]{:S(2)}) async-start(), calls=%async_computation.1 | async-start | bytes 5242880 | tf_op jit(solution)/shard_map/all_gather | solution.py:26
  8.7 275.3 %all-gather.12.cloned.1.call-start = ((), (), s32[]{:S(2)}) async-start(), calls=%async_computation.3 | async-start | bytes 5242880 | tf_op jit(solution)/shard_map/all_gather | solution.py:28
  9.3 305.5 %all-gather.14.cloned.1.call-start = ((), (), s32[]{:S(2)}) async-start(), calls=%async_computation.4 | async-start | bytes 3932160 | tf_op jit(solution)/shard_map/all_gather | solution.py:32
  122.5 80.8 %copy-start = (bf16[384,4096]{1,0:T(8,128)(2,1)S(1)}, bf16[384,4096]{1,0:T(8,128)(2,1)}, u32[]{:S(2)}) copy-start(bf16[384,4096]{1,0:T(8,128)(2,1)} %all-gather.6.cloned.1.call-done) | copy-start | bytes 9437188
  127.0 80.4 %copy-start.3 = (bf16[2,256]{1,0:T(2,128)(2,1)S(1)}, bf16[2,256]{1,0:T(2,128)(2,1)}, u32[]{:S(2)}) copy-start(bf16[2,256]{1,0:T(2,128)(2,1)} %param.16) | copy-start | bytes 3076
  206.1 2.7 collective-permute-start
  317.4 3.8 %copy-start.1 = (bf16[384,4096]{1,0:T(8,128)(2,1)S(1)}, bf16[384,4096]{1,0:T(8,128)(2,1)}, u32[]{:S(2)}) copy-start(bf16[384,4096]{1,0:T(8,128)(2,1)} %all-gather.14.cloned.1.call-done) | copy-start | bytes 9437188
  317.4 4.7 %copy-start.4 = (bf16[2,4096,256]{2,1,0:T(8,128)(2,1)S(1)}, bf16[2,4096,256]{2,1,0:T(8,128)(2,1)}, u32[]{:S(2)}) copy-start(bf16[2,4096,256]{2,1,0:T(8,128)(2,1)} %all-gather.8.cloned.1.call-done) | copy-start | bytes 12582916
  322.1 21.9 %copy-start.2 = (bf16[384,1024]{1,0:T(8,128)(2,1)S(1)}, bf16[384,1024]{1,0:T(8,128)(2,1)}, u32[]{:S(2)}) copy-start(bf16[384,1024]{1,0:T(8,128)(2,1)} %add_convert_fusion.1) | copy-start | bytes 2359300
  323.2 4.8 %collective-permute-start.1 = (bf16[30,256]{1,0:T(8,128)(2,1)S(1)}, bf16[30,256]{1,0:T(8,128)(2,1)S(1)}, u32[]{:S(2)}, u32[]{:S(2)}) collective-permute-start(bf16[30,256]{1,0:T(8,128)(2,1)S(1)} %slice.718), channel_id=1, source_target_pairs={{0,4},{4,8},{8,12},{1,5},{5,9},{9,13},{2,6},{6,10},{10,14},{3,7},{... | collective-permute-start | bytes 46088 | tf_op jit(solution)/shard_map/ppermute | solution.py:13
Sparse Core Ops, SparseCore 0:
  8.9 31.2 all-gather.5
  41.7 80.7 all-gather.9
  124.1 79.2 all-gather.7
  204.8 79.2 all-gather.11
  287.8 26.9 all-gather.13
where the time goes:
time: 355 us; the launch traced here: 354 us
  waiting for transfers between devices  275 us (77%)
  blocking collectives  28.5 us (8%)
  matrix products  19.1 us (5%)
  between operations  13.3 us (4%)
  other arithmetic  12.7 us (4%)
  starting transfers between devices  4.83 us (1%)
    all_gather x1, waiting for transfers between devices, shards(): lax.all_gather(w_gate, 'sp', axis=1, tiled=True)  79.8 us
    all_gather x1, waiting for transfers between devices, shards(): lax.all_gather(w_signal, 'sp', axis=1, tiled=True)  76.4 us
    all_gather x1, waiting for transfers between devices, shards(): lax.all_gather(w_out, 'sp', axis=1, tiled=True)  58.4 us
    all_gather x2, waiting for transfers between devices, shards(): features = lax.all_gather(current, 'tp', axis=1, tiled=True)  54.7 us
    dot_general x6, matrix products, product(): return jnp.dot(left, right, preferred_element_type=jnp.float32)  19.1 us
    all_gather x2, blocking collectives, shards(): channels = lax.all_gather(activated, 'tp', axis=1, tiled=True)  16.7 us
    psum x2, blocking collectives, shards(): lax.psum((jnp.sum(filtered, axis=-1), jnp.sum(filtered * filtered, axis=-...  11.8 us
  transfers between devices with their start and end apart: 7, of which 7 were waited for; matrix products, arithmetic and copies ran while one was open for 4% of the time, Pallas kernels for 0%

commit v1 on v0

--- a/solution.py
+++ b/solution.py
@@ -29,7 +29,14 @@
     )
     current = stream
     for layer_index in range(layer_count):
-        features = lax.all_gather(current, "tp", axis=1, tiled=True)
+        ring = [current]
+        for hop in range(3):
+            ring.append(lax.ppermute(ring[-1], "tp", [(dev, (dev + 1) % 4) for dev in range(4)]))
+        features = jnp.roll(
+            jnp.concatenate(ring[::-1], axis=1),
+            (lax.axis_index("tp") + 1) * ring[0].shape[1],
+            axis=1,
+        )
         widened = features.astype(jnp.float32)
         normed = (
             widened

time: 355 us -> 330 us (0.930)
  waiting for transfers between devices: 275 us -> 249 us
  other arithmetic: 12.7 us -> 19.1 us
  matrix products: 19.1 us -> 14.3 us
    ppermute x0 -> x6, waiting for transfers between devices: none -> 65.2 us  [shards(): lax.ppermute(ring[-1], 'tp', [(dev, (dev + 1) % 4) for dev in range(4)])]
    all_gather x2 -> x0, waiting for transfers between devices: 54.7 us -> none  [shards(): features = lax.all_gather(current, 'tp', axis=1, tiled=True)]
    all_gather x1, waiting for transfers between devices: 79.8 us -> 43.2 us  [shards(): lax.all_gather(w_gate, 'sp', axis=1, tiled=True)]
    reduce_sum x2, other arithmetic: 5.16 us -> 11.5 us  [shards(): jnp.mean(widened * widened, axis=-1, keepdims=True) + EPS]
    dot_general x6, matrix products: 19.1 us -> 14.3 us  [product(): return jnp.dot(left, right, preferred_element_type=jnp.float32)]
  transfers between devices with their start and end apart: 7 -> 11, of which waited for: 7 -> 11; matrix products, arithmetic and copies ran while one was open for 4% -> 5% of each run, Pallas kernels for 0% -> 0%
where the time goes in v1:
time: 330 us; the launch traced here: 329 us
  waiting for transfers between devices  249 us (75%)
  blocking collectives  29.2 us (9%)
  other arithmetic  19.1 us (6%)
  matrix products  14.3 us (4%)
  between operations  13.3 us (4%)
  starting transfers between devices  3.49 us (1%)
    all_gather x1, waiting for transfers between devices, shards(): lax.all_gather(w_signal, 'sp', axis=1, tiled=True)  77.4 us
    ppermute x6, waiting for transfers between devices, shards(): lax.ppermute(ring[-1], 'tp', [(dev, (dev + 1) % 4) for dev in range(4)])  65.2 us
    all_gather x1, waiting for transfers between devices, shards(): lax.all_gather(w_out, 'sp', axis=1, tiled=True)  58.6 us
    all_gather x1, waiting for transfers between devices, shards(): lax.all_gather(w_gate, 'sp', axis=1, tiled=True)  43.2 us
    all_gather x2, blocking collectives, shards(): channels = lax.all_gather(activated, 'tp', axis=1, tiled=True)  17.6 us
    dot_general x6, matrix products, product(): return jnp.dot(left, right, preferred_element_type=jnp.float32)  14.3 us
    reduce_sum x2, other arithmetic, shards(): jnp.mean(widened * widened, axis=-1, keepdims=True) + EPS  11.5 us
    psum x2, blocking collectives, shards(): lax.psum((jnp.sum(filtered, axis=-1), jnp.sum(filtered * filtered, axis=-...  11.5 us
  transfers between devices with their start and end apart: 11, of which 11 were waited for; matrix products, arithmetic and copies ran while one was open for 5% of the time, Pallas kernels for 0%

profile of v1, /device:TPU:0, one launch (start us, length us, event | category | flops | bytes accessed | tf_op | source)
XLA Modules:
  0.0 329.3 jit_solution(5296614960775955543)
XLA Ops:
  8.7 0.8 slice_convert_fusion.6
  9.5 10.9 %collective-permute-done = bf16[384,1024]{1,0:T(8,128)(2,1)S(1)} collective-permute-done((bf16[384,1024]{1,0:T(8,128)(2,1)}, bf16[384,1024]{1,0:T(8,128)(2,1)S(1)}, u32[]{:S(2)}, u32[]{:S(2)}) %collective-permute-start) | collective-permute-done | bytes 786464 | tf_op jit(solution)/shard_map/ppermute | solution.py:34
  20.4 0.8 slice_convert_fusion.5
  21.2 0.9 slice_convert_fusion
  22.1 9.7 %collective-permute-done.1 = bf16[384,1024]{1,0:T(8,128)(2,1)S(1)} collective-permute-done((bf16[384,1024]{1,0:T(8,128)(2,1)S(1)}, bf16[384,1024]{1,0:T(8,128)(2,1)S(1)}, u32[]{:S(2)}, u32[]{:S(2)}) %collective-permute-start.1) | collective-permute-done | bytes 786464 | tf_op jit(solution)/shard_map/ppermute | solution.py:34
  31.8 0.8 slice_convert_fusion.2
  32.8 10.5 %collective-permute-done.2 = bf16[384,1024]{1,0:T(8,128)(2,1)S(1)} collective-permute-done((bf16[384,1024]{1,0:T(8,128)(2,1)S(1)}, bf16[384,1024]{1,0:T(8,128)(2,1)S(1)}, u32[]{:S(2)}, u32[]{:S(2)}) %collective-permute-start.2) | collective-permute-done | bytes 786464 | tf_op jit(solution)/shard_map/ppermute | solution.py:34
  43.2 6.0 %fusion = (f32[384]{0:T(512)S(1)}, bf16[384,4096]{1,0:T(8,128)(2,1)S(1)}) fusion(s32[]{:T(128)S(6)} %select_n.13, bf16[384,1024]{1,0:T(8,128)(2,1)} %param.11, bf16[384,1024]{1,0:T(8,128)(2,1)} %copy-done, bf16[384,1024]{1,0:T(8,128)(2,1)} %copy-done.1, bf16[384,1024]{1,0:T(8,128)(2,1)S(1)} %collective-permute-done.2), kind=kLoop, calls=%fused_computation.4 | loop fusion | flops 29884032 | bytes 6292996 | tf_op jit(solution)/shard_map/reduce_sum | solution.py:43
  49.2 43.2 %all-gather.6.cloned.1.call-done = bf16[2,4096,256]{2,1,0:T(8,128)(2,1)} async-done(((bf16[2,1024,256]{2,1,0:T(8,128)(2,1)}), bf16[2,4096,256]{2,1,0:T(8,128)(2,1)}) %all-gather.6.cloned.1.call-update) | async-done | bytes 4194320 | tf_op jit(solution)/shard_map/all_gather | solution.py:27
  92.4 3.4 %fusion.35 = f32[384,256]{1,0:T(8,128)} fusion(bf16[2,4096,256]{2,1,0:T(8,128)(2,1)} %all-gather.6.cloned.1.call-done, bf16[384,4096]{1,0:T(8,128)(2,1)S(1)} %get-tuple-element.19, f32[4096]{0:T(1024)S(1)} %bitcast.120, f32[384]{0:T(512)S(1)} %add_rsqrt_fusion.3), kind=kOutput, calls=%fused_computation.121 | convolution fusion | flops 811892736 | bytes 5654016 | tf_op jit(solution)/shard_map/dot_general | solution.py:17
  95.8 77.4 %all-gather.4.cloned.1.call-done = bf16[2,4096,256]{2,1,0:T(8,128)(2,1)} async-done(((bf16[2,1024,256]{2,1,0:T(8,128)(2,1)}), bf16[2,4096,256]{2,1,0:T(8,128)(2,1)}) %all-gather.4.cloned.1.call-update) | async-done | bytes 4194320 | tf_op jit(solution)/shard_map/all_gather | solution.py:26
  173.2 2.7 fusion.37
  175.9 1.3 collective-permute-start.3
  177.2 1.4 collective-permute-done.3
  178.6 1.9 fusion.101
  180.5 5.9 %all-reduce.1 = (f32[384]{0:T(512)S(1)}, f32[384]{0:T(512)S(1)}) all-reduce(f32[384]{0:T(512)S(1)} %get-tuple-element.9, f32[384]{0:T(512)S(1)} %get-tuple-element.8), channel_id=1, replica_groups=mesh['grp'=2,'sp'=4,'tp'=4] {'tp'}, use_global_device_ids=true, to_apply=%region_4.6 | all-reduce | flops 768 | bytes 6144 | tf_op jit(solution)/shard_map/psum | solution.py:60
  186.6 8.8 %all_gather.17 = bf16[384,1024]{1,0:T(8,128)(2,1)S(1)} all-gather(bf16[384,256]{1,0:T(8,128)(2,1)S(1)} %multiply_convert_fusion.1), channel_id=1, replica_groups=mesh['grp'=2,'sp'=4,'tp'=4] {'tp'}, dimensions={1}, use_global_device_ids=true | all-gather | bytes 983040 | tf_op jit(solution)/shard_map/all_gather | solution.py:67
  195.4 58.6 %all-gather.8.cloned.1.call-done = bf16[2,1024,1024]{2,1,0:T(8,128)(2,1)} async-done(((bf16[2,256,1024]{2,1,0:T(8,128)(2,1)}), bf16[2,1024,1024]{2,1,0:T(8,128)(2,1)}) %all-gather.8.cloned.1.call-update) | async-done | bytes 4194320 | tf_op jit(solution)/shard_map/all_gather | solution.py:28
  254.1 2.7 add_convert_fusion.1
  256.9 11.4 %collective-permute-done.4 = bf16[384,1024]{1,0:T(8,128)(2,1)S(1)} collective-permute-done((bf16[384,1024]{1,0:T(8,128)(2,1)S(1)}, bf16[384,1024]{1,0:T(8,128)(2,1)S(1)}, u32[]{:S(2)}, u32[]{:S(2)}) %collective-permute-start.4) | collective-permute-done | bytes 786464 | tf_op jit(solution)/shard_map/ppermute | solution.py:34
  268.3 11.4 %collective-permute-done.5 = bf16[384,1024]{1,0:T(8,128)(2,1)S(1)} collective-permute-done((bf16[384,1024]{1,0:T(8,128)(2,1)S(1)}, bf16[384,1024]{1,0:T(8,128)(2,1)S(1)}, u32[]{:S(2)}, u32[]{:S(2)}) %collective-permute-start.5) | collective-permute-done | bytes 786464 | tf_op jit(solution)/shard_map/ppermute | solution.py:34
  279.7 11.4 %collective-permute-done.6 = bf16[384,1024]{1,0:T(8,128)(2,1)S(1)} collective-permute-done((bf16[384,1024]{1,0:T(8,128)(2,1)S(1)}, bf16[384,1024]{1,0:T(8,128)(2,1)S(1)}, u32[]{:S(2)}, u32[]{:S(2)}) %collective-permute-start.6) | collective-permute-done | bytes 786464 | tf_op jit(solution)/shard_map/ppermute | solution.py:34
  291.1 5.6 %fusion.3 = (f32[384]{0:T(512)S(1)}, bf16[384,4096]{1,0:T(8,128)(2,1)S(1)}) fusion(s32[]{:T(128)S(6)} %select_n.13, bf16[384,1024]{1,0:T(8,128)(2,1)S(1)} %add_convert_fusion.1, bf16[384,1024]{1,0:T(8,128)(2,1)S(1)} %collective-permute-done.4, bf16[384,1024]{1,0:T(8,128)(2,1)S(1)} %collective-permute-done.5, bf16[384,1024]{1,0:T(8,128)(2,1)S(1)} %collective-permute-done.6), kind=kLoop, calls=%fused_computation.7 | loop fusion | flops 29884032 | bytes 6292996 | tf_op jit(solution)/shard_map/reduce_sum | solution.py:43
  296.7 1.1 fusion.33
  297.8 1.1 copy-done.4
  298.9 1.0 fusion.36
  300.0 1.5 collective-permute-start.7
  301.5 1.2 collective-permute-done.7
  302.7 1.9 fusion.100
  304.6 5.7 %all-reduce = (f32[384]{0:T(512)S(1)}, f32[384]{0:T(512)S(1)}) all-reduce(f32[384]{0:T(512)S(1)} %get-tuple-element.7, f32[384]{0:T(512)S(1)} %get-tuple-element.6), channel_id=1, replica_groups=mesh['grp'=2,'sp'=4,'tp'=4] {'tp'}, use_global_device_ids=true, to_apply=%region_9.11 | all-reduce | flops 768 | bytes 6144 | tf_op jit(solution)/shard_map/psum | solution.py:60
  310.5 8.8 %all_gather.19 = bf16[384,1024]{1,0:T(8,128)(2,1)S(1)} all-gather(bf16[384,256]{1,0:T(8,128)(2,1)S(1)} %multiply_convert_fusion), channel_id=1, replica_groups=mesh['grp'=2,'sp'=4,'tp'=4] {'tp'}, dimensions={1}, use_global_device_ids=true | all-gather | bytes 983040 | tf_op jit(solution)/shard_map/all_gather | solution.py:67
  319.3 3.5 %add_convert_fusion = bf16[384,1024]{1,0:T(8,128)(2,1)} fusion(bf16[384,1024]{1,0:T(8,128)(2,1)S(1)} %add_convert_fusion.1, bf16[384,1024]{1,0:T(8,128)(2,1)S(1)} %all_gather.19, bf16[2,1024,1024]{2,1,0:T(8,128)(2,1)} %all-gather.8.cloned.1.call-done), kind=kOutput, calls=%fused_computation.110 | convolution fusion | flops 806486016 | bytes 4456448 | tf_op jit(solution)/shard_map/dot_general | solution.py:17
  (34 shorter events, 2.9 us)
Async XLA Ops:
  6.5 85.9 %all-gather.6.cloned.1.call-start = ((), (), s32[]{:S(2)}) async-start(), calls=%async_computation.1 | async-start | bytes 5242880 | tf_op jit(solution)/shard_map/all_gather | solution.py:27
  7.3 166.0 %all-gather.4.cloned.1.call-start = ((), (), s32[]{:S(2)}) async-start(), calls=%async_computation | async-start | bytes 5242880 | tf_op jit(solution)/shard_map/all_gather | solution.py:26
  8.0 246.1 %all-gather.8.cloned.1.call-start = ((), (), s32[]{:S(2)}) async-start(), calls=%async_computation.2 | async-start | bytes 5242880 | tf_op jit(solution)/shard_map/all_gather | solution.py:28
  8.1 12.3 %collective-permute-start = (bf16[384,1024]{1,0:T(8,128)(2,1)}, bf16[384,1024]{1,0:T(8,128)(2,1)S(1)}, u32[]{:S(2)}, u32[]{:S(2)}) collective-permute-start(bf16[384,1024]{1,0:T(8,128)(2,1)} %param.11), channel_id=1, source_target_pairs={{0,1},{1,2},{2,3},{3,0},{4,5},{5,6},{6,7},{7,4},{8,9},{9,10},{10,1... | collective-permute-start | bytes 2359304 | tf_op jit(solution)/shard_map/ppermute | solution.py:34
  20.4 12.3 %copy-start = (bf16[384,1024]{1,0:T(8,128)(2,1)}, bf16[384,1024]{1,0:T(8,128)(2,1)S(1)}, u32[]{:S(2)}) copy-start(bf16[384,1024]{1,0:T(8,128)(2,1)S(1)} %collective-permute-done) | copy-start | bytes 2359300
  20.4 11.4 %collective-permute-start.1 = (bf16[384,1024]{1,0:T(8,128)(2,1)S(1)}, bf16[384,1024]{1,0:T(8,128)(2,1)S(1)}, u32[]{:S(2)}, u32[]{:S(2)}) collective-permute-start(bf16[384,1024]{1,0:T(8,128)(2,1)S(1)} %collective-permute-done), channel_id=1, source_target_pairs={{0,1},{1,2},{2,3},{3,0},{4,5},{5,6},{6,7},{7,4},{8,9},{9,10},{10,1... | collective-permute-start | bytes 2359304 | tf_op jit(solution)/shard_map/ppermute | solution.py:34
  31.8 1.0 copy-start.1
  31.8 11.4 %collective-permute-start.2 = (bf16[384,1024]{1,0:T(8,128)(2,1)S(1)}, bf16[384,1024]{1,0:T(8,128)(2,1)S(1)}, u32[]{:S(2)}, u32[]{:S(2)}) collective-permute-start(bf16[384,1024]{1,0:T(8,128)(2,1)S(1)} %collective-permute-done.1), channel_id=1, source_target_pairs={{0,1},{1,2},{2,3},{3,0},{4,5},{5,6},{6,7},{7,4},{8,9},{9,10},{10,1... | collective-permute-start | bytes 2359304 | tf_op jit(solution)/shard_map/ppermute | solution.py:34
  95.8 81.4 %copy-start.2 = (bf16[2,256]{1,0:T(2,128)(2,1)S(1)}, bf16[2,256]{1,0:T(2,128)(2,1)}, u32[]{:S(2)}) copy-start(bf16[2,256]{1,0:T(2,128)(2,1)} %param.18) | copy-start | bytes 3076
  175.9 2.7 collective-permute-start.3
  256.8 39.9 %copy-start.3 = (bf16[2,4096,256]{2,1,0:T(8,128)(2,1)S(1)}, bf16[2,4096,256]{2,1,0:T(8,128)(2,1)}, u32[]{:S(2)}) copy-start(bf16[2,4096,256]{2,1,0:T(8,128)(2,1)} %all-gather.6.cloned.1.call-done) | copy-start | bytes 12582916
  256.8 11.5 %collective-permute-start.4 = (bf16[384,1024]{1,0:T(8,128)(2,1)S(1)}, bf16[384,1024]{1,0:T(8,128)(2,1)S(1)}, u32[]{:S(2)}, u32[]{:S(2)}) collective-permute-start(bf16[384,1024]{1,0:T(8,128)(2,1)S(1)} %add_convert_fusion.1), channel_id=1, source_target_pairs={{0,1},{1,2},{2,3},{3,0},{4,5},{5,6},{6,7},{7,4},{8,9},{9,10},{10,1... | collective-permute-start | bytes 2359304 | tf_op jit(solution)/shard_map/ppermute | solution.py:34
  268.3 11.4 %collective-permute-start.5 = (bf16[384,1024]{1,0:T(8,128)(2,1)S(1)}, bf16[384,1024]{1,0:T(8,128)(2,1)S(1)}, u32[]{:S(2)}, u32[]{:S(2)}) collective-permute-start(bf16[384,1024]{1,0:T(8,128)(2,1)S(1)} %collective-permute-done.4), channel_id=1, source_target_pairs={{0,1},{1,2},{2,3},{3,0},{4,5},{5,6},{6,7},{7,4},{8,9},{9,10},{10,1... | collective-permute-start | bytes 2359304 | tf_op jit(solution)/shard_map/ppermute | solution.py:34
  279.7 11.4 %collective-permute-start.6 = (bf16[384,1024]{1,0:T(8,128)(2,1)S(1)}, bf16[384,1024]{1,0:T(8,128)(2,1)S(1)}, u32[]{:S(2)}, u32[]{:S(2)}) collective-permute-start(bf16[384,1024]{1,0:T(8,128)(2,1)S(1)} %collective-permute-done.5), channel_id=1, source_target_pairs={{0,1},{1,2},{2,3},{3,0},{4,5},{5,6},{6,7},{7,4},{8,9},{9,10},{10,1... | collective-permute-start | bytes 2359304 | tf_op jit(solution)/shard_map/ppermute | solution.py:34
  296.7 2.2 copy-start.4
  300.0 2.7 collective-permute-start.7
Sparse Core Ops, SparseCore 0:
  8.9 83.4 all-gather.5
  94.0 79.2 all-gather.3
  174.8 79.2 all-gather.7
